TPU v7x, 32 devices: a whole 2x2x4 slice. The times are simulated.
32 devices in a mesh: ep: 16 (over z, y, core), tp: 2 (over x).
Axes of the slice: x: 2, y: 2, z: 4, core: 2. Of those that a mesh axis runs over, the one named last changes fastest.
Arguments:
- tokens: bfloat16 [256, 2048], P('ep'), may hold values from -6 to 6
- recur_state: float32 [256, 8, 128, 128], P('ep', 'tp'), may hold values from -0.4 to 0.4
- attn_gain: float32 [2048], replicated, may hold values from 0.1 to 1.9
- query_weight: bfloat16 [2048, 1024], P(None, 'tp'), may hold values from -0.125 to 0.125
- key_weight: bfloat16 [2048, 1024], P(None, 'tp'), may hold values from -0.125 to 0.125
- value_weight: bfloat16 [2048, 1024], P(None, 'tp'), may hold values from -0.125 to 0.125
- outgate_weight: bfloat16 [2048, 1024], P(None, 'tp'), may hold values from -0.125 to 0.125
- beta_weight: bfloat16 [2048, 8], replicated, may hold values from -0.125 to 0.125
- decay_weight: bfloat16 [2048, 8], replicated, may hold values from -0.125 to 0.125
- decay_rate: float32 [8], replicated, may hold values from 0.05 to 2
- head_gain: float32 [128], replicated, may hold values from 0.1 to 1.9
- output_weight: bfloat16 [1024, 2048], P('tp'), may hold values from -0.1875 to 0.1875
- ffn_gain: float32 [2048], replicated, may hold values from 0.1 to 1.9
- routes: int32 [256, 2], P('ep'), may hold values from 0 to 3, all different within a row; in each aligned block of 16 rows (0 to 15, 16 to 31, ...) at most 16 rows name the same one
- route_weight: float32 [256, 2], P('ep'), may hold values from 0.2 to 1
- expert_gate: bfloat16 [16, 2048, 1024], P('ep', None, 'tp'), may hold values from -0.125 to 0.125
- expert_up: bfloat16 [16, 2048, 1024], P('ep', None, 'tp'), may hold values from -0.125 to 0.125
- expert_down: bfloat16 [16, 1024, 2048], P('ep', 'tp'), may hold values from -0.09375 to 0.09375
Outputs:
- mixed: bfloat16 [256, 2048], P('ep', 'tp')
- new_state: float32 [256, 8, 128, 128], P('ep', 'tp')
Inputs may be any that keep to these rules, and one draw needn't show every extreme that they name: `routes`: each row names 2 different experts; in each aligned block of 16 rows no expert is named by more than 16 rows.
All inputs are finite; a program needn't handle non-finite values.
Results may differ from a plain program's by a relative error of at most 0.014.
Values may be sent and summed in bfloat16 or wider, within the bound.
A program may use at most 64 MiB of HBM per device.

v0:
```python
import jax
import jax.numpy as jnp
from jax import lax
from jax.sharding import PartitionSpec as P

EPS = 1e-06


def rms_scale(values, gain):
    return values * lax.rsqrt(jnp.mean(values * values, axis=-1, keepdims=True) + EPS) * gain


def unit_rows(values):
    return values * lax.rsqrt(jnp.sum(values * values, axis=-1, keepdims=True) + EPS)


def slot_targets(group_routes, experts, capacity):
    flat = group_routes.reshape(-1)
    onehot = (flat[:, None] == jnp.arange(experts, dtype=jnp.int32)[None, :]).astype(jnp.int32)
    running = jnp.cumsum(onehot, axis=0)
    position = jnp.sum(running * onehot, axis=1) - 1
    return (flat * capacity + position).reshape(group_routes.shape)


def local(
    tokens,
    recur_state,
    attn_gain,
    query_weight,
    key_weight,
    value_weight,
    outgate_weight,
    beta_weight,
    decay_weight,
    decay_rate,
    head_gain,
    output_weight,
    ffn_gain,
    routes,
    route_weight,
    expert_gate,
    expert_up,
    expert_down,
):
    f32 = jnp.float32
    bf16 = jnp.bfloat16
    highest = lax.Precision.HIGHEST
    seq_count, model_width = tokens.shape
    heads_here = recur_state.shape[1]
    head_size = recur_state.shape[2]
    groups = lax.axis_size("ep")
    lanes = lax.axis_size("tp")
    lane_index = lax.axis_index("tp")
    normed = rms_scale(tokens.astype(f32), attn_gain).astype(bf16)
    qproj = jnp.dot(normed, query_weight, preferred_element_type=f32).astype(bf16)
    kproj = jnp.dot(normed, key_weight, preferred_element_type=f32).astype(bf16)
    vproj = jnp.dot(normed, value_weight, preferred_element_type=f32).astype(bf16)
    zproj = jnp.dot(normed, outgate_weight, preferred_element_type=f32).astype(bf16)
    first_head = lane_index * heads_here
    own_beta = lax.dynamic_slice_in_dim(beta_weight, first_head, heads_here, 1)
    own_decay = lax.dynamic_slice_in_dim(decay_weight, first_head, heads_here, 1)
    own_rate = lax.dynamic_slice_in_dim(decay_rate, first_head, heads_here, 0)
    strength = jax.nn.sigmoid(jnp.dot(normed, own_beta, preferred_element_type=f32))
    fading = jnp.exp(
        -own_rate * jax.nn.softplus(jnp.dot(normed, own_decay, preferred_element_type=f32))
    )

    def split_heads(proj):
        return proj.astype(f32).reshape(seq_count, heads_here, head_size)

    query = unit_rows(jax.nn.silu(split_heads(qproj))) * head_size ** (-0.5)
    keyvec = unit_rows(jax.nn.silu(split_heads(kproj)))
    value = jax.nn.silu(split_heads(vproj))
    recall = jnp.einsum("thd,thde->the", keyvec, recur_state, precision=highest)
    written = (strength[..., None] * keyvec)[..., :, None] * (value - fading[..., None] * recall)[
        ..., None, :
    ]
    new_state = fading[..., None, None] * recur_state + written
    readout = jnp.einsum("thd,thde->the", query, new_state, precision=highest)
    headed = (
        (rms_scale(readout, head_gain) * jax.nn.silu(split_heads(zproj)))
        .reshape(seq_count, heads_here * head_size)
        .astype(bf16)
    )
    partial_out = jnp.dot(headed, output_weight, preferred_element_type=f32)
    branch = lax.psum(partial_out, "tp").astype(bf16)
    resid = (tokens.astype(f32) + branch.astype(f32)).astype(bf16)
    ffn_in = rms_scale(resid.astype(f32), ffn_gain).astype(bf16)
    top_count = routes.shape[1]
    experts = groups // 4
    capacity = min(seq_count, max(2, (2 * seq_count * top_count + experts - 1) // experts))
    quarter = model_width // lanes
    targets = slot_targets(routes, experts, capacity)
    slot_ids = jnp.arange(experts * capacity, dtype=jnp.int32)
    select = jnp.any(slot_ids[:, None, None] == targets[None, :, :], axis=-1).astype(bf16)
    gate_local = expert_gate[0]
    up_local = expert_up[0]
    down_local = expert_down[0]
    packed = jnp.dot(select, ffn_in, preferred_element_type=f32).astype(bf16)
    packed = packed.reshape(experts, 1, capacity, ffn_in.shape[1])
    packed = jnp.broadcast_to(packed, (experts, 4, capacity, ffn_in.shape[1]))
    arrived = lax.all_to_all(
        packed.reshape(groups, capacity, ffn_in.shape[1]),
        "ep",
        split_axis=0,
        concat_axis=0,
        tiled=True,
    ).reshape(groups * capacity, model_width)
    gated = jnp.dot(arrived, gate_local, preferred_element_type=f32)
    lifted = jnp.dot(arrived, up_local, preferred_element_type=f32)
    hidden = (jax.nn.silu(gated) * lifted).astype(bf16)
    slice_terms = jnp.dot(hidden, down_local, preferred_element_type=f32).reshape(
        groups, capacity, model_width
    )
    shares = lax.psum_scatter(slice_terms, "tp", scatter_dimension=2, tiled=True).astype(bf16)
    returned = lax.all_to_all(shares, "ep", split_axis=0, concat_axis=0, tiled=True)
    merged = (
        returned.astype(f32)
        .reshape(experts, 4, capacity, quarter)
        .sum(axis=1)
        .reshape(experts * capacity, quarter)
    )
    combine = jnp.zeros((seq_count, experts * capacity), f32)
    for choice_idx in range(top_count):
        match = (targets[:, choice_idx, None] == slot_ids[None, :]).astype(f32)
        combine = combine + route_weight[:, choice_idx, None] * match
    moe = jnp.dot(combine, merged, precision=highest)
    resid_own = lax.dynamic_slice_in_dim(resid, lane_index * quarter, quarter, 1)
    mixed = (resid_own.astype(f32) + moe).astype(bf16)
    return (mixed, new_state)


def solution(mesh):
    return jax.shard_map(
        local,
        mesh=mesh,
        in_specs=(
            P("ep", None),
            P("ep", "tp", None, None),
            P(),
            P(None, "tp"),
            P(None, "tp"),
            P(None, "tp"),
            P(None, "tp"),
            P(),
            P(),
            P(),
            P(),
            P("tp", None),
            P(),
            P("ep", None),
            P("ep", None),
            P("ep", None, "tp"),
            P("ep", None, "tp"),
            P("ep", "tp", None),
        ),
        out_specs=(P("ep", "tp"), P("ep", "tp", None, None)),
        check_vma=False,
    )
```

profile of v0, /device:TPU:0, one launch (start us, length us, event | category | flops | bytes accessed | tf_op | source)
XLA Modules:
  0.0 138.9 jit_solution(11278963235603328612)
XLA Ops:
  7.3 1.1 fusion.23
  8.4 1.1 fusion.19
  9.5 2.1 %fusion.15 = f32[16,512]{1,0:T(8,128)S(1)} fusion(bf16[2048,512]{1,0:T(8,128)(2,1)} %param.22, bf16[16,2048]{1,0:T(8,128)(2,1)} %param.18, f32[2048]{0:T(1024)} %param.20, f32[16]{0:T(128)S(1)} %add_rsqrt_fusion.4), kind=kOutput, calls=%fused_computation.17 | convolution fusion | flops 33701888 | bytes 2203712 | tf_op jit(solution)/shard_map/dot_general | solution.py:56
  11.9 0.2 fusion.50
  12.2 2.0 %fusion.14 = f32[16,512]{1,0:T(8,128)S(1)} fusion(bf16[2048,512]{1,0:T(8,128)(2,1)} %param.23, bf16[16,2048]{1,0:T(8,128)(2,1)S(1)} %copy-done.3, f32[2048]{0:T(1024)S(1)} %copy-done.5, f32[16]{0:T(128)S(1)} %add_rsqrt_fusion.4), kind=kOutput, calls=%fused_computation.15 | convolution fusion | flops 33701888 | bytes 2203712 | tf_op jit(solution)/shard_map/dot_general | solution.py:57
  14.2 2.0 %fusion.16 = f32[16,512]{1,0:T(8,128)S(1)} fusion(bf16[2048,512]{1,0:T(8,128)(2,1)} %param.21, bf16[16,2048]{1,0:T(8,128)(2,1)S(1)} %copy-done.3, f32[2048]{0:T(1024)S(1)} %copy-done.5, f32[16]{0:T(128)S(1)} %add_rsqrt_fusion.4), kind=kOutput, calls=%fused_computation.19 | convolution fusion | flops 33701888 | bytes 2203712 | tf_op jit(solution)/shard_map/dot_general | solution.py:55
  16.6 5.5 %fusion.63 = f32[16,4,1,128]{3,2,1,0:T(1,128)S(1)} fusion(f32[16,4,128,1]{2,3,1,0:T(1,128)S(1)} %bitcast.66, f32[16,4,128,128]{3,2,1,0:T(8,128)} %param.19), kind=kOutput, calls=%fused_computation.91 | convolution fusion | flops 12582912 | bytes 4259840 | tf_op jit(solution)/shard_map/thd,thde->the/dot_general | solution.py:74
  22.2 1.5 %multiply_add_fusion = f32[16,4,128,128]{3,2,1,0:T(8,128)S(1)} fusion(f32[16,4,128,128]{3,2,1,0:T(8,128)S(1)} %copy-done.1, f32[16,4,128]{2,1,0:T(4,128)S(1)} %fusion.30, f32[16,4,128]{2,1,0:T(4,128)S(1)} %get-tuple-element.4, f32[16,4]{1,0:T(8,128)S(1)} %copy.39), kind=kLoop, calls=%fused_computation | loop fusion | flops 3145728 | bytes 8454400 | tf_op jit(solution)/shard_map/add | solution.py:78
  23.7 3.7 %fusion.64 = f32[16,4,1,128]{3,2,1,0:T(1,128)S(1)} fusion(f32[16,4,128,1]{2,3,1,0:T(1,128)S(1)} %bitcast.67, f32[16,4,128,128]{3,2,1,0:T(8,128)S(1)} %multiply_add_fusion), kind=kOutput, calls=%fused_computation.92 | convolution fusion | flops 12582912 | bytes 4259840 | tf_op jit(solution)/shard_map/thd,thde->the/dot_general | solution.py:79
  27.5 0.4 fusion.13
  28.1 2.0 %fusion.33 = f32[16,2048]{1,0:T(8,128)S(1)} fusion(bf16[512,2048]{1,0:T(8,128)(2,1)} %param.29, bf16[2,8,4,128]{3,2,1,0:T(4,128)(2,1)S(1)} %bitcast.69), kind=kOutput, calls=%fused_computation.50 | convolution fusion | flops 33554432 | bytes 2244608 | tf_op jit(solution)/shard_map/dot_general | solution.py:85
  30.1 11.3 %all-reduce.1 = bf16[16,2048]{1,0:T(8,128)(2,1)S(1)} all-reduce(f32[16,2048]{1,0:T(8,128)S(1)} %fusion.33), channel_id=1, replica_groups=mesh['ep'=16,'tp'=2] {'tp'}, use_global_device_ids=true, to_apply=%region_4.5 | all-reduce | flops 32768 | bytes 196608 | tf_op jit(solution)/shard_map/psum | solution.py:86
  41.9 0.2 select_reduce_fusion
  42.4 0.3 convolution_convert_fusion
  42.8 30.4 %all_to_all.10 = bf16[16,16,2048]{2,1,0:T(8,128)(2,1)S(1)} all-to-all(bf16[16,16,2048]{2,1,0:T(8,128)(2,1)S(1)} %bitcast.58), channel_id=1, replica_groups=mesh['ep'=16,'tp'=2] {'ep'}, dimensions={0} | all-to-all | bytes 2097152 | tf_op jit(solution)/shard_map/all_to_all | solution.py:102
  73.2 0.7 fusion.4
  73.9 0.9 copy-done.11
  74.7 0.7 fusion.9
  75.5 2.1 %fusion = f32[16,16,2048]{2,1,0:T(8,128)} fusion(bf16[16,16,512]{2,1,0:T(8,128)(2,1)S(1)} %bitcast.65, bf16[1,512,2048]{2,1,0:T(8,128)(2,1)S(1)} %copy-done), kind=kOutput, calls=%fused_computation.2 | convolution fusion | flops 536870912 | bytes 4456448 | tf_op jit(solution)/shard_map/dot_general | solution.py:112
  77.6 31.5 %reduce-scatter.2.cloned.1.call-done = f32[16,16,1024]{2,1,0:T(8,128)} async-done(((f32[16,16,2048]{2,1,0:T(8,128)}), f32[16,16,1024]{2,1,0:T(8,128)}) %reduce-scatter.2.cloned.1.call-update) | async-done | bytes 1048592 | tf_op jit(solution)/shard_map/reduce_scatter | solution.py:115
  109.1 2.1 %convert_element_type.83 = bf16[16,16,1024]{2,1,0:T(8,128)(2,1)} convert(f32[16,16,1024]{2,1,0:T(8,128)} %reduce-scatter.2.cloned.1.call-done) | non-fusion elementwise | flops 262144 | bytes 1572864 | tf_op jit(solution)/shard_map/convert_element_type | solution.py:115
  111.2 5.6 %all-to-all-start.1 = ((bf16[16,16,1024]{2,1,0:T(8,128)(2,1)}), bf16[16,16,1024]{2,1,0:T(8,128)(2,1)S(1)}, u32[]{:S(2)}, u32[]{:S(2)}) async-start(bf16[16,16,1024]{2,1,0:T(8,128)(2,1)} %convert_element_type.83), calls=%async_computation.2 | async-start | bytes 1048576 | tf_op jit(solution)/shard_map/all_to_all | solution.py:116
  116.8 14.2 %all-to-all-done.1 = bf16[16,16,1024]{2,1,0:T(8,128)(2,1)S(1)} async-done(((bf16[16,16,1024]{2,1,0:T(8,128)(2,1)}), bf16[16,16,1024]{2,1,0:T(8,128)(2,1)S(1)}, u32[]{:S(2)}, u32[]{:S(2)}) %all-to-all-start.1) | async-done | bytes 524320 | tf_op jit(solution)/shard_map/all_to_all | solution.py:116
  131.1 0.9 fusion.12
  (62 shorter events, 2.1 us)
Async XLA Ops:
  7.2 68.3 %copy-start = (bf16[1,512,2048]{2,1,0:T(8,128)(2,1)S(1)}, bf16[1,512,2048]{2,1,0:T(8,128)(2,1)}, u32[]{:S(2)}) copy-start(bf16[1,512,2048]{2,1,0:T(8,128)(2,1)} %param.35) | copy-start | bytes 6291460
  7.2 4.7 %copy-start.3 = (bf16[16,2048]{1,0:T(8,128)(2,1)S(1)}, bf16[16,2048]{1,0:T(8,128)(2,1)}, u32[]{:S(2)}) copy-start(bf16[16,2048]{1,0:T(8,128)(2,1)} %param.18) | copy-start | bytes 196612
  7.2 4.7 %copy-start.5 = (f32[2048]{0:T(1024)S(1)}, f32[2048]{0:T(1024)}, u32[]{:S(2)}) copy-start(f32[2048]{0:T(1024)} %param.20) | copy-start | bytes 24580
  7.2 4.6 %copy-start.13 = (f32[8]{0:T(128)S(1)}, f32[8]{0:T(128)}, u32[]{:S(2)}) copy-start(f32[8]{0:T(128)} %param.27) | copy-start | bytes 100
  7.2 4.7 %copy-start.12 = (bf16[2048,8]{0,1:T(8,128)(2,1)S(1)}, bf16[2048,8]{0,1:T(8,128)(2,1)}, u32[]{:S(2)}) copy-start(bf16[2048,8]{0,1:T(8,128)(2,1)} %param.26) | copy-start | bytes 98308
  7.2 101.8 %reduce-scatter.2.cloned.1.call-start = ((), (), s32[]{:S(2)}) async-start(), calls=%async_computation.3 | async-start | bytes 3145728 | tf_op jit(solution)/shard_map/reduce_scatter | solution.py:115
  16.6 5.6 %copy-start.1 = (f32[16,4,128,128]{3,2,1,0:T(8,128)S(1)}, f32[16,4,128,128]{3,2,1,0:T(8,128)}, u32[]{:S(2)}) copy-start(f32[16,4,128,128]{3,2,1,0:T(8,128)} %param.19) | copy-start | bytes 12582916
  23.7 3.7 %copy-start.2 = (f32[16,4,128,128]{3,2,1,0:T(8,128)}, f32[16,4,128,128]{3,2,1,0:T(8,128)S(1)}, u32[]{:S(2)}) copy-start(f32[16,4,128,128]{3,2,1,0:T(8,128)S(1)} %multiply_add_fusion) | copy-start | bytes 12582916
  23.7 3.8 %copy-start.4 = (bf16[2048,512]{1,0:T(8,128)(2,1)S(1)}, bf16[2048,512]{1,0:T(8,128)(2,1)}, u32[]{:S(2)}) copy-start(bf16[2048,512]{1,0:T(8,128)(2,1)} %param.24) | copy-start | bytes 6291460
  27.4 0.7 copy-start.9
  27.5 14.1 %copy-start.7 = (s32[16,2]{0,1:T(2,128)S(1)}, s32[16,2]{0,1:T(2,128)}, u32[]{:S(2)}) copy-start(s32[16,2]{0,1:T(2,128)} %param.31) | copy-start | bytes 388
  27.5 14.9 %copy-start.6 = (f32[2048]{0:T(1024)S(1)}, f32[2048]{0:T(1024)}, u32[]{:S(2)}) copy-start(f32[2048]{0:T(1024)} %param.30) | copy-start | bytes 24580
  42.3 30.9 %copy-start.10 = (bf16[1,2048,512]{2,1,0:T(8,128)(2,1)S(1)}, bf16[1,2048,512]{2,1,0:T(8,128)(2,1)}, u32[]{:S(2)}) copy-start(bf16[1,2048,512]{2,1,0:T(8,128)(2,1)} %param.33) | copy-start | bytes 6291460
  73.2 1.6 %copy-start.11 = (bf16[1,2048,512]{2,1,0:T(8,128)(2,1)S(1)}, bf16[1,2048,512]{2,1,0:T(8,128)(2,1)}, u32[]{:S(2)}) copy-start(bf16[1,2048,512]{2,1,0:T(8,128)(2,1)} %param.34) | copy-start | bytes 6291460
  77.5 39.3 %copy-start.8 = (f32[16,2]{0,1:T(2,128)S(1)}, f32[16,2]{0,1:T(2,128)}, u32[]{:S(2)}) copy-start(f32[16,2]{0,1:T(2,128)} %param.32) | copy-start | bytes 388
  111.2 19.9 %all-to-all-start.1 = ((bf16[16,16,1024]{2,1,0:T(8,128)(2,1)}), bf16[16,16,1024]{2,1,0:T(8,128)(2,1)S(1)}, u32[]{:S(2)}, u32[]{:S(2)}) async-start(bf16[16,16,1024]{2,1,0:T(8,128)(2,1)} %convert_element_type.83), calls=%async_computation.2 | async-start | bytes 1048576 | tf_op jit(solution)/shard_map/all_to_all | solution.py:116
Sparse Core Ops, SparseCore 0:
  77.7 31.3 reduce-scatter.1
where the time goes:
time: 139 us
  waiting for transfers between devices  45.8 us (33%)
  blocking collectives  41.7 us (30%)
  matrix products  23.6 us (17%)
  between operations  14.3 us (10%)
  other arithmetic  6.09 us (4%)
  starting transfers between devices  5.65 us (4%)
  local copies, waits for them, and re-layouts  1.71 us (1%)
    reduce_scatter x1, waiting for transfers between devices, local(): lax.psum_scatter(slice_terms, 'tp', scatter_dimension=2, tiled=True)  31.5 us
    all_to_all x1, blocking collectives, local(): lax.all_to_all(packed.reshape(groups, capacity, ffn_in.shape[1]), 'ep', s...  30.4 us
    all_to_all x1, waiting for transfers between devices, local(): lax.all_to_all(shares, 'ep', split_axis=0, concat_axis=0, tiled=True)  14.2 us
    psum x1, blocking collectives, local(): branch = lax.psum(partial_out, 'tp').astype(bf16)  11.3 us
    all_to_all x1, starting transfers between devices, local(): lax.all_to_all(shares, 'ep', split_axis=0, concat_axis=0, tiled=True)  5.61 us
    dot_general x1, matrix products, local(): recall = jnp.einsum('thd,thde->the', keyvec, recur_state, precision=highest)  5.48 us
    dot_general x1, matrix products, local(): readout = jnp.einsum('thd,thde->the', query, new_state, precision=highest)  3.66 us
  transfers between devices with their start and end apart: 2, of which 2 were waited for; matrix products, arithmetic and copies ran while one was open for 0% of the time, Pallas kernels for 0%

commit v1 on v0

v1 whole, which is shorter than its diff:
```python
import functools

import jax
import jax.numpy as jnp
from jax import lax
from jax.experimental import pallas as pl
from jax.experimental.pallas import tpu as pltpu
from jax.sharding import PartitionSpec as P

EPS = 1e-06
MESH = pl.DeviceIdType.MESH
F32 = jnp.float32
BF16 = jnp.bfloat16
SIDE = 128


def silu(values):
    return values / (1.0 + jnp.exp(-values))


def unit_rows(values):
    return values * lax.rsqrt(jnp.sum(values * values, axis=-1, keepdims=True) + EPS)


def rms_scale(values, gain):
    return values * lax.rsqrt(jnp.mean(values * values, axis=-1, keepdims=True) + EPS) * gain


def mixer_kernel(
    tok_ref, gain_ref, bt_ref, dt_ref, rate_ref, hg_ref,
    wk_hbm, wq_hbm, wv_hbm, st_hbm, wz_hbm, wo_hbm,
    out_ref, ns_hbm,
    wk, wq, wv, wz, wo, st, ns, w_sem, s_sem, n_sem,
):
    heads, seqs, hd = st.shape[0], st.shape[1], st.shape[2]

    def fetch(src, dst, i):
        copy = pltpu.make_async_copy(src, dst, w_sem.at[i])
        copy.start()
        return copy

    ck, cq, cv = fetch(wk_hbm, wk, 0), fetch(wq_hbm, wq, 1), fetch(wv_hbm, wv, 2)
    cs = []
    for j in range(heads):
        copy = pltpu.make_async_copy(st_hbm.at[:, j], st.at[j], s_sem.at[j])
        copy.start()
        cs.append(copy)
    cz, co = fetch(wz_hbm, wz, 3), fetch(wo_hbm, wo, 4)

    normed = rms_scale(tok_ref[...].astype(F32), gain_ref[...]).astype(BF16)
    dims = (((1,), (1,)), ((), ()))
    bl = lax.dot_general(normed, bt_ref[...], dims, preferred_element_type=F32)
    dl = lax.dot_general(normed, dt_ref[...], dims, preferred_element_type=F32)
    strength = 1.0 / (1.0 + jnp.exp(-bl))
    softplus = jnp.maximum(dl, 0.0) + jnp.log1p(jnp.exp(-jnp.abs(dl)))
    fading = jnp.exp(-rate_ref[...] * softplus)
    first = lax.axis_index("tp") * heads
    head_ids = lax.broadcasted_iota(jnp.int32, bl.shape, 1)

    def own(values, j):
        return jnp.sum(jnp.where(head_ids == first + j, values, 0.0), axis=1, keepdims=True)

    def project(copy, ref):
        copy.wait()
        return jnp.dot(normed, ref[...], preferred_element_type=F32).astype(BF16).astype(F32)

    kp, qp, vp = project(ck, wk), project(cq, wq), project(cv, wv)
    row2 = lax.broadcasted_iota(jnp.int32, (2 * seqs, hd), 0)
    row1 = lax.broadcasted_iota(jnp.int32, (seqs, hd), 0)
    outs, readouts = [], []
    for j in range(heads):
        cut = slice(j * hd, (j + 1) * hd)
        kh = unit_rows(silu(kp[:, cut]))
        qh = unit_rows(silu(qp[:, cut])) * hd ** (-0.5)
        vh = silu(vp[:, cut])
        both = jnp.concatenate([kh, qh], axis=0)
        spread = jnp.concatenate(
            [jnp.where((row2 == t) | (row2 == t + seqs), both, 0.0).astype(BF16) for t in range(seqs)],
            axis=1,
        )
        cs[j].wait()
        held = st[j].reshape(seqs * hd, hd).astype(BF16)
        read = jnp.dot(spread, held, preferred_element_type=F32)
        fd, bt = own(fading, j), own(strength, j)
        delta = bt * (vh - fd * read[:seqs])
        readouts.append(fd * read[seqs:] + jnp.sum(kh * qh, axis=-1, keepdims=True) * delta)
        kt = kh.T.astype(BF16)
        fdb = jnp.broadcast_to(fd, (seqs, hd))
        step = 4
        for t0 in range(0, seqs, step):
            block = jnp.concatenate(
                [jnp.where(row1 == t, delta, 0.0).astype(BF16) for t in range(t0, t0 + step)], axis=1
            )
            written = jnp.dot(kt, block, preferred_element_type=F32)
            for i in range(step):
                t = t0 + i
                ns[j, t] = fdb[t : t + 1] * st[j, t] + written[:, i * hd : (i + 1) * hd]
        copy = pltpu.make_async_copy(ns.at[j], ns_hbm.at[:, j], n_sem.at[j])
        copy.start()
        outs.append(copy)
    zp = project(cz, wz)
    headed = jnp.concatenate(
        [
            (rms_scale(readouts[j], hg_ref[...]) * silu(zp[:, j * hd : (j + 1) * hd])).astype(BF16)
            for j in range(heads)
        ],
        axis=1,
    )
    co.wait()
    out_ref[...] = jnp.dot(headed, wo[...], preferred_element_type=F32).astype(BF16)
    for copy in outs:
        copy.wait()


def expert_kernel(
    nz, ny, lanes,
    tok_ref, part_ref, gain_ref, routes_ref, rw_ref, wg_hbm, wu_hbm, wd_hbm,
    out_ref,
    wg, wu, wd, tpb, rows, resid, cs, cr, pf, xs, xr, qf, ys, yr, zs, zr,
    w_sem, tp_s, tp_r, ag_s, ag_r, c_s, c_r, x_s, x_r, y_s, y_r, z_s, z_r,
):
    seqs, width = tok_ref.shape
    dl = width // lanes
    zy = nz * ny
    ep, tp = lax.axis_index("ep"), lax.axis_index("tp")
    c = lax.rem(ep, 2)
    y = lax.rem(ep // 2, ny)
    z = ep // (2 * ny)
    other = 1 - c

    fetched = []
    for i, (src, dst) in enumerate(((wg_hbm, wg), (wu_hbm, wu), (wd_hbm, wd))):
        copy = pltpu.make_async_copy(src.at[0], dst, w_sem.at[i])
        copy.start()
        fetched.append(copy)

    def device(zz, yy, cc):
        return {"ep": (zz * ny + yy) * 2 + cc}

    def turn(base, step, size):
        return lax.rem(base + step, size)

    partner = device(z, y, other)
    barrier = pltpu.get_barrier_semaphore()
    peers = [partner]
    peers += [{"tp": turn(tp, d, lanes)} for d in range(1, lanes)]
    peers += [device(z, turn(y, d, ny), c) for d in range(1, ny)]
    peers += [device(turn(z, d, nz), y, c) for d in range(1, nz)]
    for peer in peers:
        pl.semaphore_signal(barrier, inc=1, device_id=peer, device_id_type=MESH)
    pl.semaphore_wait(barrier, len(peers))

    started = []

    def remote(src, dst, s_sem, r_sem, dev):
        return pltpu.make_async_remote_copy(
            src_ref=src, dst_ref=dst, send_sem=s_sem, recv_sem=r_sem, device_id=dev, device_id_type=MESH
        )

    def send(src, dst, s_sem, r_sem, dev):
        copy = remote(src, dst, s_sem, r_sem, dev)
        copy.start()
        started.append(copy)

    def arrive(dst, s_sem, r_sem):
        remote(dst, dst, s_sem, r_sem, partner).wait_recv()

    for d in range(1, lanes):
        send(part_ref, tpb.at[tp], tp_s.at[d], tp_r.at[tp], {"tp": turn(tp, d, lanes)})

    routes, weights = routes_ref[...], rw_ref[...]
    side = lax.broadcasted_iota(jnp.int32, (seqs, SIDE), 1)
    expert_of = jnp.where(side >= SIDE // 2, side - SIDE // 2, side)
    combine = jnp.zeros((seqs, SIDE), F32)
    for k in range(routes.shape[1]):
        combine = combine + jnp.where(expert_of == routes[:, k : k + 1], weights[:, k : k + 1], 0.0)
    high = combine.astype(BF16).astype(F32)
    packed = jnp.where(side >= SIDE // 2, combine - high, high).astype(BF16)

    branch = part_ref[...].astype(F32)
    for d in range(1, lanes):
        src = turn(tp, d, lanes)
        arrive(tpb.at[src], tp_s.at[0], tp_r.at[src])
        branch = branch + tpb[src].astype(F32)
    res = (tok_ref[...].astype(F32) + branch.astype(BF16).astype(F32)).astype(BF16).astype(F32)
    for j in range(lanes):
        resid[j] = res[:, j * dl : (j + 1) * dl]

    def place(zz, yy, cc):
        return cc * zy + zz * ny + yy

    mine = place(z, y, c)
    rows[mine, :, :width] = rms_scale(res, gain_ref[...]).astype(BF16)
    rows[mine, :, width:] = packed

    count = [0]

    def pass_on(p, dev):
        send(rows.at[p], rows.at[p], ag_s.at[count[0]], ag_r.at[p], dev)
        count[0] += 1

    def landed(p):
        arrive(rows.at[p], ag_s.at[0], ag_r.at[p])

    near = sorted(range(1, nz), key=lambda d: (min(d, nz - d), d))
    for d in reversed(near):
        pass_on(mine, device(turn(z, d, nz), y, c))
    for d in range(1, ny):
        pass_on(mine, device(z, turn(y, d, ny), c))
    pass_on(mine, partner)
    for dz in near:
        p = place(turn(z, dz, nz), y, c)
        landed(p)
        for d in range(1, ny):
            pass_on(p, device(z, turn(y, d, ny), c))
        pass_on(p, partner)
    for dz in [0] + near:
        for d in range(1, ny):
            p = place(turn(z, dz, nz), turn(y, d, ny), c)
            landed(p)
            pass_on(p, partner)

    my_expert = ep // 4
    lane_id = lax.broadcasted_iota(jnp.int32, (zy * seqs, SIDE), 1)

    def hidden_of(half):
        block = rows[pl.ds(half * zy, zy)].reshape(zy * seqs, width + SIDE)
        x = block[:, :width]
        pick = (lane_id == my_expert) | (lane_id == my_expert + SIDE // 2)
        share = jnp.sum(jnp.where(pick, block[:, width:].astype(F32), 0.0), axis=1, keepdims=True)
        gated = jnp.dot(x, wg[...], preferred_element_type=F32)
        lifted = jnp.dot(x, wu[...], preferred_element_type=F32)
        return (silu(gated) * lifted * share).astype(BF16)

    fetched[0].wait()
    fetched[1].wait()
    hidden_own = hidden_of(c)
    for dz in [0] + near:
        for d in range(ny):
            landed(place(turn(z, dz, nz), turn(y, d, ny), other))
    hidden_far = hidden_of(other)
    fetched[2].wait()
    for j in range(lanes):
        cut = slice(j * dl, (j + 1) * dl)
        far = jnp.dot(hidden_far, wd[:, cut], preferred_element_type=F32)
        cs[j] = far.astype(BF16).reshape(zy, seqs, dl)

    order = list(reversed(near)) + [0]

    def chunk(k):
        zt = turn(z, k, nz)
        return zt, pl.ds(zt * ny, ny)

    for k in order:
        _, at = chunk(k)
        send(cs.at[:, at], cr.at[:, at], c_s.at[k], c_r.at[k], partner)
    for j in range(lanes):
        cut = slice(j * dl, (j + 1) * dl)
        near_half = jnp.dot(hidden_own, wd[:, cut], preferred_element_type=F32)
        pf[j] = near_half.reshape(zy, seqs, dl)
    for k in order:
        _, at = chunk(k)
        arrive(cr.at[:, at], c_s.at[k], c_r.at[k])
        for d in range(1, lanes):
            jt = turn(tp, d, lanes)
            xs[jt, at] = (pf[jt, at] + cr[jt, at].astype(F32)).astype(BF16)
            send(xs.at[jt, at], xr.at[tp, at], x_s.at[d, k], x_r.at[tp, k], {"tp": jt})
        pf[tp, at] = pf[tp, at] + cr[tp, at].astype(F32)
    for k in order:
        zt, at = chunk(k)
        total = pf[tp, at]
        for d in range(1, lanes):
            src = turn(tp, d, lanes)
            arrive(xr.at[src, at], x_s.at[d, k], x_r.at[src, k])
            total = total + xr[src, at].astype(F32)
        qf[at] = total
        for d in range(1, ny):
            yt = turn(y, d, ny)
            ys[zt * ny + yt] = qf[zt * ny + yt].astype(BF16)
            send(ys.at[zt * ny + yt], yr.at[zt * ny + y], y_s.at[d, k], y_r.at[y, k], device(z, yt, c))
    for k in order:
        zt, at = chunk(k)
        total = qf[zt * ny + y]
        for d in range(1, ny):
            src = turn(y, d, ny)
            arrive(yr.at[zt * ny + src], y_s.at[d, k], y_r.at[src, k])
            total = total + yr[zt * ny + src].astype(F32)
        if k:
            zs[zt] = total.astype(BF16)
            send(zs.at[zt], zr.at[z], z_s.at[k], z_r.at[z], device(zt, y, c))
    for d in near:
        src = turn(z, d, nz)
        arrive(zr.at[src], z_s.at[d], z_r.at[src])
        total = total + zr[src].astype(F32)
    out_ref[...] = (resid[tp] + total).astype(BF16)
    for copy in started:
        copy.wait_send()


def local(
    tokens, recur_state, attn_gain, query_weight, key_weight, value_weight, outgate_weight,
    beta_weight, decay_weight, decay_rate, head_gain, output_weight, ffn_gain, routes,
    route_weight, expert_gate, expert_up, expert_down,
):
    seqs, width = tokens.shape
    heads, hd = recur_state.shape[1], recur_state.shape[2]
    groups, lanes = lax.axis_size("ep"), lax.axis_size("tp")
    ny = 1
    while ny * ny * 4 <= groups // 2:
        ny *= 2
    nz = groups // (2 * ny)
    zy = nz * ny
    dl = width // lanes
    hidden = expert_gate.shape[2]
    vmem = pl.BlockSpec(memory_space=pltpu.VMEM)
    any_ = pl.BlockSpec(memory_space=pl.ANY)
    dma = pltpu.SemaphoreType.DMA
    inner = heads * hd
    part, new_state = pl.pallas_call(
        mixer_kernel,
        name="mixer",
        out_shape=(
            jax.ShapeDtypeStruct((seqs, width), BF16),
            jax.ShapeDtypeStruct(recur_state.shape, F32),
        ),
        in_specs=[vmem] * 6 + [any_] * 6,
        out_specs=(vmem, any_),
        scratch_shapes=[pltpu.VMEM((width, inner), BF16)] * 4
        + [
            pltpu.VMEM((inner, width), BF16),
            pltpu.VMEM((heads, seqs, hd, hd), F32),
            pltpu.VMEM((heads, seqs, hd, hd), F32),
            dma((5,)),
            dma((heads,)),
            dma((heads,)),
        ],
        compiler_params=pltpu.CompilerParams(vmem_limit_bytes=60 * 1024 * 1024),
    )(
        tokens, attn_gain[None], beta_weight.T, decay_weight.T, decay_rate[None], head_gain[None],
        key_weight, query_weight, value_weight, recur_state, outgate_weight, output_weight,
    )
    mixed = pl.pallas_call(
        functools.partial(expert_kernel, nz, ny, lanes),
        name="experts",
        out_shape=jax.ShapeDtypeStruct((seqs, dl), BF16),
        in_specs=[vmem] * 5 + [any_] * 3,
        out_specs=vmem,
        scratch_shapes=[
            pltpu.VMEM((width, hidden), BF16),
            pltpu.VMEM((width, hidden), BF16),
            pltpu.VMEM((hidden, width), BF16),
            pltpu.VMEM((lanes, seqs, width), BF16),
            pltpu.VMEM((groups, seqs, width + SIDE), BF16),
            pltpu.VMEM((lanes, seqs, dl), F32),
            pltpu.VMEM((lanes, zy, seqs, dl), BF16),
            pltpu.VMEM((lanes, zy, seqs, dl), BF16),
            pltpu.VMEM((lanes, zy, seqs, dl), F32),
            pltpu.VMEM((lanes, zy, seqs, dl), BF16),
            pltpu.VMEM((lanes, zy, seqs, dl), BF16),
            pltpu.VMEM((zy, seqs, dl), F32),
            pltpu.VMEM((zy, seqs, dl), BF16),
            pltpu.VMEM((zy, seqs, dl), BF16),
            pltpu.VMEM((nz, seqs, dl), BF16),
            pltpu.VMEM((nz, seqs, dl), BF16),
            dma((3,)),
            dma((lanes,)),
            dma((lanes,)),
            dma((groups,)),
            dma((groups,)),
            dma((nz,)),
            dma((nz,)),
            dma((lanes, nz)),
            dma((lanes, nz)),
            dma((ny, nz)),
            dma((ny, nz)),
            dma((nz,)),
            dma((nz,)),
        ],
        compiler_params=pltpu.CompilerParams(
            collective_id=0, has_side_effects=True, vmem_limit_bytes=60 * 1024 * 1024
        ),
    )(
        tokens, part, ffn_gain[None], routes, route_weight, expert_gate, expert_up, expert_down,
    )
    return mixed, new_state


def solution(mesh):
    return jax.shard_map(
        local,
        mesh=mesh,
        in_specs=(
            P("ep", None),
            P("ep", "tp", None, None),
            P(),
            P(None, "tp"),
            P(None, "tp"),
            P(None, "tp"),
            P(None, "tp"),
            P(),
            P(),
            P(),
            P(),
            P("tp", None),
            P(),
            P("ep", None),
            P("ep", None),
            P("ep", None, "tp"),
            P("ep", None, "tp"),
            P("ep", "tp", None),
        ),
        out_specs=(P("ep", "tp"), P("ep", "tp", None, None)),
        check_vma=False,
    )
```

time: 139 us -> 50.7 us (0.36)
  waiting for transfers between devices: 45.8 us -> 0 us
  Pallas kernels: 0 us -> 45.7 us
  blocking collectives: 41.7 us -> 0 us
  matrix products: 23.6 us -> 0 us
  between operations: 14.3 us -> 0.65 us
  other arithmetic: 6.09 us -> 0 us
  starting transfers between devices: 5.65 us -> 0 us
  local copies, waits for them, and re-layouts: 1.71 us -> 4.08 us
    pallas_call x0 -> x2, Pallas kernels: none -> 45.7 us  [the longest x1 37.6 us: local(): pl.pallas_call(functools.partial(expert_kernel, nz, ny, lanes), name='exp...]
    reduce_scatter x1 -> x0, waiting for transfers between devices: 31.5 us -> none  [local(): lax.psum_scatter(slice_terms, 'tp', scatter_dimension=2, tiled=True)]
    all_to_all x1 -> x0, blocking collectives: 30.4 us -> none  [local(): lax.all_to_all(packed.reshape(groups, capacity, ffn_in.shape[1]), 'ep', s...]
    dot_general x14 -> x0, matrix products: 23.6 us -> none  [the longest x1 5.48 us: local(): recall = jnp.einsum('thd,thde->the', keyvec, recur_state, precision=highest)]
    all_to_all x1 -> x0, waiting for transfers between devices: 14.2 us -> none  [local(): lax.all_to_all(shares, 'ep', split_axis=0, concat_axis=0, tiled=True)]
    psum x1 -> x0, blocking collectives: 11.3 us -> none  [local(): branch = lax.psum(partial_out, 'tp').astype(bf16)]
    all_to_all x1 -> x0, starting transfers between devices: 5.61 us -> none  [local(): lax.all_to_all(shares, 'ep', split_axis=0, concat_axis=0, tiled=True)]
    unnamed x29 -> x3, local copies, waits for them, and re-layouts: 1.1 us -> 4.08 us
  transfers between devices with their start and end apart: 2 -> 0, of which waited for: 2 -> 0; matrix products, arithmetic and copies ran while one was open for 0% -> 0% of each run, Pallas kernels for 0% -> 0%
where the time goes in v1:
time: 50.7 us; the launch traced here: 50.4 us
  Pallas kernels  45.7 us (90%)
  local copies, waits for them, and re-layouts  4.08 us (8%)
  between operations  0.65 us (1%)
    pallas_call x1, Pallas kernels, local(): pl.pallas_call(functools.partial(expert_kernel, nz, ny, lanes), name='exp...  37.6 us
    pallas_call x1, Pallas kernels, local(): pl.pallas_call(mixer_kernel, name='mixer', out_shape=(jax.ShapeDtypeStruc...  8.05 us
    unnamed x3, local copies, waits for them, and re-layouts  4.08 us

profile of v1, /device:TPU:0, one launch (start us, length us, event | category | flops | bytes accessed | tf_op | source)
XLA Modules:
  0.0 50.4 jit_solution(6211475873130130924)
XLA Ops:
  0.6 1.4 %copy.20.routes_ref = s32[16,2]{1,0:T(8,128)} copy(s32[16,2]{0,1:T(2,128)} %param.31) | data formatting | bytes 256 | tf_op args[13]
  2.0 1.4 %copy.21.rw_ref = f32[16,2]{1,0:T(8,128)} copy(f32[16,2]{0,1:T(2,128)} %param.32) | data formatting | bytes 256 | tf_op args[14]
  3.3 8.0 %mixer.1 = (bf16[16,2048]{1,0:T(8,128)(2,1)}, f32[16,4,128,128]{3,2,1,0:T(8,128)}) custom-call(bf16[16,2048]{1,0:T(8,128)(2,1)} %tok_ref.3, f32[1,2048]{1,0:T(1,128)} %bitcast.8, bf16[8,2048]{1,0:T(8,128)(2,1)} %bitcast.6, bf16[8,2048]{1,0:T(8,128)(2,1)} %bitcast.7, f32[1,8]{1,0:T(1,128)} %bitcast.10, f32[1,128]{1,0:T(1,128)} %bitcast.11, ...), custom_call_target="tpu_custom_call" | custom-call | tf_op jit(solution)/shard_map/mixer/pallas_call | solution.py:319
  11.4 37.6 %experts.1 = bf16[16,1024]{1,0:T(8,128)(2,1)} custom-call(bf16[16,2048]{1,0:T(8,128)(2,1)} %tok_ref.3, bf16[16,2048]{1,0:T(8,128)(2,1)} %get-tuple-element.4.part_ref, f32[1,2048]{1,0:T(1,128)} %bitcast.9, s32[16,2]{1,0:T(8,128)} %copy.20.routes_ref, f32[16,2]{1,0:T(8,128)} %copy.21.rw_ref, bf16[1,2048,512]{2,1,0:T(8,128)(2,1)} %wg_hbm.1, ...), custom_call_target="tpu_custom_call" | custom-call | tf_op jit(solution)/shard_map/experts/pallas_call | solution.py:342
  49.0 1.4 %copy.23 = bf16[16,1024]{1,0:T(8,128)(2,1)} copy(bf16[16,1024]{1,0:T(8,128)(2,1)} %experts.1) | data formatting | bytes 65536

commit v2 on v1

--- a/solution.py
+++ b/solution.py
@@ -116,7 +116,7 @@
     nz, ny, lanes,
     tok_ref, part_ref, gain_ref, routes_ref, rw_ref, wg_hbm, wu_hbm, wd_hbm,
     out_ref,
-    wg, wu, wd, tpb, rows, resid, cs, cr, pf, xs, xr, qf, ys, yr, zs, zr,
+    wg, wu, wd, tpb, rows, resid, cs, cr, pf, xs, xr, qf, ys, yr, ybs, ybr, zs, zr,
     w_sem, tp_s, tp_r, ag_s, ag_r, c_s, c_r, x_s, x_r, y_s, y_r, z_s, z_r,
 ):
     seqs, width = tok_ref.shape
@@ -168,12 +168,16 @@
     for d in range(1, lanes):
         send(part_ref, tpb.at[tp], tp_s.at[d], tp_r.at[tp], {"tp": turn(tp, d, lanes)})
 
-    routes, weights = routes_ref[...], rw_ref[...]
+    routes, weights = routes_ref[...].astype(F32), rw_ref[...]
+    top = routes.shape[0]
+    pad = jnp.zeros((8 - 2 * top % 8, seqs), F32)
+    turned = jnp.concatenate([routes, weights, pad], axis=0).T
     side = lax.broadcasted_iota(jnp.int32, (seqs, SIDE), 1)
-    expert_of = jnp.where(side >= SIDE // 2, side - SIDE // 2, side)
+    expert_of = jnp.where(side >= SIDE // 2, side - SIDE // 2, side).astype(F32)
     combine = jnp.zeros((seqs, SIDE), F32)
-    for k in range(routes.shape[1]):
-        combine = combine + jnp.where(expert_of == routes[:, k : k + 1], weights[:, k : k + 1], 0.0)
+    for k in range(top):
+        weight = turned[:, top + k : top + k + 1]
+        combine = combine + jnp.where(expert_of == turned[:, k : k + 1], weight, 0.0)
     high = combine.astype(BF16).astype(F32)
     packed = jnp.where(side >= SIDE // 2, combine - high, high).astype(BF16)
 
@@ -194,37 +198,70 @@
     rows[mine, :, width:] = packed
 
     count = [0]
-
-    def pass_on(p, dev):
-        send(rows.at[p], rows.at[p], ag_s.at[count[0]], ag_r.at[p], dev)
+    half = nz // 2
+    low = z < half
+    base = jnp.where(low, 0, half)
+    edge = jnp.where(low, half - 1, half)
+    far_edge = jnp.where(low, half, half - 1)
+    outward = jnp.where(low, 1, -1)
+    at_edge = z == edge
+    middle = width // 2
+    pieces = (slice(0, middle), slice(middle, width + SIDE))
+
+    def block(p, piece):
+        return rows.at[p, :, pieces[piece]]
+
+    def pass_on(p, piece, dev):
+        send(block(p, piece), block(p, piece), ag_s.at[count[0]], ag_r.at[piece, p], dev)
         count[0] += 1
 
-    def landed(p):
-        arrive(rows.at[p], ag_s.at[0], ag_r.at[p])
-
-    near = sorted(range(1, nz), key=lambda d: (min(d, nz - d), d))
-    for d in reversed(near):
-        pass_on(mine, device(turn(z, d, nz), y, c))
-    for d in range(1, ny):
-        pass_on(mine, device(z, turn(y, d, ny), c))
-    pass_on(mine, partner)
-    for dz in near:
-        p = place(turn(z, dz, nz), y, c)
-        landed(p)
+    def landed(p, piece):
+        arrive(block(p, piece), ag_s.at[0], ag_r.at[piece, p])
+
+    def spread(p, piece):
         for d in range(1, ny):
-            pass_on(p, device(z, turn(y, d, ny), c))
-        pass_on(p, partner)
-    for dz in [0] + near:
+            pass_on(p, piece, device(z, turn(y, d, ny), c))
+        pass_on(p, piece, partner)
+
+    mates = [base + lax.rem(z - base + d, half) for d in range(1, half)]
+    both = range(len(pieces))
+    for piece in both:
+        pass_on(mine, piece, device(far_edge, y, c))
+        for mate in mates:
+            pass_on(mine, piece, device(mate, y, c))
+        spread(mine, piece)
+    for mate in mates:
+        for piece in both:
+            p = place(mate, y, c)
+            landed(p, piece)
+            spread(p, piece)
+    relayed = []
+    for i in range(half):
+        for piece in both:
+            p = place(far_edge + outward * i, y, c)
+            landed(p, piece)
+            for mate in mates:
+                copy = remote(
+                    block(p, piece), block(p, piece), ag_s.at[count[0]], ag_r.at[piece, p],
+                    device(mate, y, c),
+                )
+                count[0] += 1
+                relayed.append(copy)
+                pl.when(at_edge)(copy.start)
+            spread(p, piece)
+    columns = [z] + mates + [far_edge + outward * i for i in range(half)]
+    for zz in columns:
         for d in range(1, ny):
-            p = place(turn(z, dz, nz), turn(y, d, ny), c)
-            landed(p)
-            pass_on(p, partner)
+            for piece in both:
+                p = place(zz, turn(y, d, ny), c)
+                landed(p, piece)
+                pass_on(p, piece, partner)
 
     my_expert = ep // 4
     lane_id = lax.broadcasted_iota(jnp.int32, (zy * seqs, SIDE), 1)
 
-    def hidden_of(half):
-        block = rows[pl.ds(half * zy, zy)].reshape(zy * seqs, width + SIDE)
+    def hidden_of(side_of):
+        block = rows[pl.ds(side_of * zy, zy)].reshape(zy * seqs, width + SIDE)
         x = block[:, :width]
         pick = (lane_id == my_expert) | (lane_id == my_expert + SIDE // 2)
         share = jnp.sum(jnp.where(pick, block[:, width:].astype(F32), 0.0), axis=1, keepdims=True)
@@ -235,66 +272,98 @@
     fetched[0].wait()
     fetched[1].wait()
     hidden_own = hidden_of(c)
-    for dz in [0] + near:
-        for d in range(ny):
-            landed(place(turn(z, dz, nz), turn(y, d, ny), other))
+    for d in range(ny):
+        for zz in columns:
+            for piece in both:
+                landed(place(zz, turn(y, d, ny), other), piece)
     hidden_far = hidden_of(other)
     fetched[2].wait()
+    targets = [lax.rem(z + outward * d + nz, nz) for d in range(nz - 1, -1, -1)]
+    spans = [pl.ds(zt * ny, ny) for zt in targets]
+    steps = range(nz)
     for j in range(lanes):
         cut = slice(j * dl, (j + 1) * dl)
         far = jnp.dot(hidden_far, wd[:, cut], preferred_element_type=F32)
         cs[j] = far.astype(BF16).reshape(zy, seqs, dl)
-
-    order = list(reversed(near)) + [0]
-
-    def chunk(k):
-        zt = turn(z, k, nz)
-        return zt, pl.ds(zt * ny, ny)
-
-    for k in order:
-        _, at = chunk(k)
-        send(cs.at[:, at], cr.at[:, at], c_s.at[k], c_r.at[k], partner)
+        for i in steps:
+            send(cs.at[j, spans[i]], cr.at[j, spans[i]], c_s.at[j, i], c_r.at[j, i], partner)
     for j in range(lanes):
         cut = slice(j * dl, (j + 1) * dl)
         near_half = jnp.dot(hidden_own, wd[:, cut], preferred_element_type=F32)
         pf[j] = near_half.reshape(zy, seqs, dl)
-    for k in order:
-        _, at = chunk(k)
-        arrive(cr.at[:, at], c_s.at[k], c_r.at[k])
-        for d in range(1, lanes):
-            jt = turn(tp, d, lanes)
-            xs[jt, at] = (pf[jt, at] + cr[jt, at].astype(F32)).astype(BF16)
-            send(xs.at[jt, at], xr.at[tp, at], x_s.at[d, k], x_r.at[tp, k], {"tp": jt})
-        pf[tp, at] = pf[tp, at] + cr[tp, at].astype(F32)
-    for k in order:
-        zt, at = chunk(k)
-        total = pf[tp, at]
-        for d in range(1, lanes):
-            src = turn(tp, d, lanes)
-            arrive(xr.at[src, at], x_s.at[d, k], x_r.at[src, k])
-            total = total + xr[src, at].astype(F32)
-        qf[at] = total
-        for d in range(1, ny):
-            yt = turn(y, d, ny)
-            ys[zt * ny + yt] = qf[zt * ny + yt].astype(BF16)
-            send(ys.at[zt * ny + yt], yr.at[zt * ny + y], y_s.at[d, k], y_r.at[y, k], device(z, yt, c))
-    for k in order:
-        zt, at = chunk(k)
-        total = qf[zt * ny + y]
-        for d in range(1, ny):
-            src = turn(y, d, ny)
-            arrive(yr.at[zt * ny + src], y_s.at[d, k], y_r.at[src, k])
-            total = total + yr[zt * ny + src].astype(F32)
-        if k:
+
+    def first_tp(i):
+        return i % 2 == 0
+
+    tp_peers = [(d, turn(tp, d, lanes)) for d in range(1, lanes)]
+    y_peers = [(d, turn(y, d, ny)) for d in range(1, ny)]
+    for i in steps:
+        zt, at = targets[i], spans[i]
+        for j in range(lanes):
+            arrive(cr.at[j, at], c_s.at[j, i], c_r.at[j, i])
+        if first_tp(i):
+            for d, jt in tp_peers:
+                xs[jt, at] = (pf[jt, at] + cr[jt, at].astype(F32)).astype(BF16)
+                send(xs.at[jt, at], xr.at[tp, at], x_s.at[d, i], x_r.at[tp, i], {"tp": jt})
+            pf[tp, at] = pf[tp, at] + cr[tp, at].astype(F32)
+        else:
+            for d, yt in y_peers:
+                row = zt * ny + yt
+                ybs[:, row] = (pf[:, row] + cr[:, row].astype(F32)).astype(BF16)
+                send(
+                    ybs.at[:, row], ybr.at[:, zt * ny + y], y_s.at[d, i], y_r.at[y, i], device(z, yt, c)
+                )
+            row = zt * ny + y
+            pf[:, row] = pf[:, row] + cr[:, row].astype(F32)
+    for i in steps:
+        zt, at = targets[i], spans[i]
+        if first_tp(i):
+            total = pf[tp, at]
+            for d, src in tp_peers:
+                arrive(xr.at[src, at], x_s.at[d, i], x_r.at[src, i])
+                total = total + xr[src, at].astype(F32)
+            qf[at] = total
+            for d, yt in y_peers:
+                row = zt * ny + yt
+                ys[row] = qf[row].astype(BF16)
+                send(ys.at[row], yr.at[zt * ny + y], y_s.at[d, i], y_r.at[y, i], device(z, yt, c))
+        else:
+            row = zt * ny + y
+            total = pf[:, row]
+            for d, src in y_peers:
+                back = zt * ny + src
+                arrive(ybr.at[:, back], y_s.at[d, i], y_r.at[src, i])
+                total = total + ybr[:, back].astype(F32)
+            pf[:, row] = total
+            for d, jt in tp_peers:
+                xs[jt, row] = pf[jt, row].astype(BF16)
+                send(xs.at[jt, row], xr.at[tp, row], x_s.at[d, i], x_r.at[tp, i], {"tp": jt})
+    for i in steps:
+        zt = targets[i]
+        row = zt * ny + y
+        if first_tp(i):
+            total = qf[row]
+            for d, src in y_peers:
+                back = zt * ny + src
+                arrive(yr.at[back], y_s.at[d, i], y_r.at[src, i])
+                total = total + yr[back].astype(F32)
+        else:
+            total = pf[tp, row]
+            for d, src in tp_peers:
+                arrive(xr.at[src, row], x_s.at[d, i], x_r.at[src, i])
+                total = total + xr[src, row].astype(F32)
+        if i < nz - 1:
             zs[zt] = total.astype(BF16)
-            send(zs.at[zt], zr.at[z], z_s.at[k], z_r.at[z], device(zt, y, c))
-    for d in near:
+            send(zs.at[zt], zr.at[z], z_s.at[i], z_r.at[z], device(zt, y, c))
+    for d in range(1, nz):
         src = turn(z, d, nz)
-        arrive(zr.at[src], z_s.at[d], z_r.at[src])
+        arrive(zr.at[src], z_s.at[0], z_r.at[src])
         total = total + zr[src].astype(F32)
     out_ref[...] = (resid[tp] + total).astype(BF16)
     for copy in started:
         copy.wait_send()
+    for copy in relayed:
+        pl.when(at_edge)(copy.wait_send)
 
 
 def local(
@@ -360,15 +429,17 @@
             pltpu.VMEM((zy, seqs, dl), F32),
             pltpu.VMEM((zy, seqs, dl), BF16),
             pltpu.VMEM((zy, seqs, dl), BF16),
+            pltpu.VMEM((lanes, zy, seqs, dl), BF16),
+            pltpu.VMEM((lanes, zy, seqs, dl), BF16),
             pltpu.VMEM((nz, seqs, dl), BF16),
             pltpu.VMEM((nz, seqs, dl), BF16),
             dma((3,)),
             dma((lanes,)),
             dma((lanes,)),
-            dma((groups,)),
-            dma((groups,)),
-            dma((nz,)),
-            dma((nz,)),
+            dma((2 * (nz // 2) ** 2 + 2 * nz * (ny - 1) + 2 * zy,)),
+            dma((2, groups)),
+            dma((lanes, nz)),
+            dma((lanes, nz)),
             dma((lanes, nz)),
             dma((lanes, nz)),
             dma((ny, nz)),
@@ -380,7 +451,7 @@
             collective_id=0, has_side_effects=True, vmem_limit_bytes=60 * 1024 * 1024
         ),
     )(
-        tokens, part, ffn_gain[None], routes, route_weight, expert_gate, expert_up, expert_down,
+        tokens, part, ffn_gain[None], routes.T, route_weight.T, expert_gate, expert_up, expert_down,
     )
     return mixed, new_state
 

time: 50.7 us -> 46.3 us (0.913)
  local copies, waits for them, and re-layouts: 4.08 us -> 1.38 us
  Pallas kernels: 45.7 us -> 44 us
    unnamed x3 -> x1, local copies, waits for them, and re-layouts: 4.08 us -> 1.38 us
    pallas_call x1, Pallas kernels: 37.6 us -> 35.9 us  [local(): pl.pallas_call(functools.partial(expert_kernel, nz, ny, lanes), name='exp...]
where the time goes in v2:
time: 46.3 us; the launch traced here: 46 us
  Pallas kernels  44 us (95%)
  local copies, waits for them, and re-layouts  1.38 us (3%)
  between operations  0.65 us (1%)
    pallas_call x1, Pallas kernels, local(): pl.pallas_call(functools.partial(expert_kernel, nz, ny, lanes), name='exp...  35.9 us
    pallas_call x1, Pallas kernels, local(): pl.pallas_call(mixer_kernel, name='mixer', out_shape=(jax.ShapeDtypeStruc...  8.05 us
    unnamed x1, local copies, waits for them, and re-layouts  1.38 us

profile of v2, /device:TPU:0, one launch (start us, length us, event | category | flops | bytes accessed | tf_op | source)
XLA Modules:
  0.0 46.0 jit_solution(8483286285969505837)
XLA Ops:
  0.6 8.1 %mixer.1 = (bf16[16,2048]{1,0:T(8,128)(2,1)}, f32[16,4,128,128]{3,2,1,0:T(8,128)}) custom-call(bf16[16,2048]{1,0:T(8,128)(2,1)} %tok_ref.3, f32[1,2048]{1,0:T(1,128)} %bitcast.10, bf16[8,2048]{1,0:T(8,128)(2,1)} %bitcast.8, bf16[8,2048]{1,0:T(8,128)(2,1)} %bitcast.9, f32[1,8]{1,0:T(1,128)} %bitcast.14, f32[1,128]{1,0:T(1,128)} %bitcast.15, ...), custom_call_target="tpu_custom_call" | custom-call | tf_op jit(solution)/shard_map/mixer/pallas_call | solution.py:388
  8.7 35.9 %experts.1 = bf16[16,1024]{1,0:T(8,128)(2,1)} custom-call(bf16[16,2048]{1,0:T(8,128)(2,1)} %tok_ref.3, bf16[16,2048]{1,0:T(8,128)(2,1)} %get-tuple-element.4.part_ref, f32[1,2048]{1,0:T(1,128)} %bitcast.11, s32[2,16]{1,0:T(2,128)} %bitcast.12, f32[2,16]{1,0:T(2,128)} %bitcast.13, bf16[1,2048,512]{2,1,0:T(8,128)(2,1)} %wg_hbm.1, ...), custom_call_target="tpu_custom_call" | custom-call | tf_op jit(solution)/shard_map/experts/pallas_call | solution.py:411
  44.6 1.4 %copy.21 = bf16[16,1024]{1,0:T(8,128)(2,1)} copy(bf16[16,1024]{1,0:T(8,128)(2,1)} %experts.1) | data formatting | bytes 65536

commit v3 on v2

--- a/solution.py
+++ b/solution.py
@@ -27,9 +27,10 @@
 
 
 def mixer_kernel(
-    tok_ref, gain_ref, bt_ref, dt_ref, rate_ref, hg_ref,
+    tok_hbm, gain_hbm, bt_hbm, dt_hbm, rate_hbm, hg_hbm,
     wk_hbm, wq_hbm, wv_hbm, st_hbm, wz_hbm, wo_hbm,
     out_ref, ns_hbm,
+    tok_ref, gain_ref, bt_ref, dt_ref, rate_ref, hg_ref,
     wk, wq, wv, wz, wo, st, ns, w_sem, s_sem, n_sem,
 ):
     heads, seqs, hd = st.shape[0], st.shape[1], st.shape[2]
@@ -39,6 +40,11 @@
         copy.start()
         return copy
 
+    small = (
+        (tok_hbm, tok_ref), (gain_hbm, gain_ref), (bt_hbm, bt_ref),
+        (dt_hbm, dt_ref), (rate_hbm, rate_ref), (hg_hbm, hg_ref),
+    )
+    first_in = [fetch(src, dst, 5 + i) for i, (src, dst) in enumerate(small)]
     ck, cq, cv = fetch(wk_hbm, wk, 0), fetch(wq_hbm, wq, 1), fetch(wv_hbm, wv, 2)
     cs = []
     for j in range(heads):
@@ -47,6 +53,8 @@
         cs.append(copy)
     cz, co = fetch(wz_hbm, wz, 3), fetch(wo_hbm, wo, 4)
 
+    for copy in first_in:
+        copy.wait()
     normed = rms_scale(tok_ref[...].astype(F32), gain_ref[...]).astype(BF16)
     dims = (((1,), (1,)), ((), ()))
     bl = lax.dot_general(normed, bt_ref[...], dims, preferred_element_type=F32)
@@ -385,33 +393,36 @@
     any_ = pl.BlockSpec(memory_space=pl.ANY)
     dma = pltpu.SemaphoreType.DMA
     inner = heads * hd
+    smalls = (
+        tokens, attn_gain[None], beta_weight.T, decay_weight.T, decay_rate[None], head_gain[None],
+    )
     part, new_state = pl.pallas_call(
         mixer_kernel,
         name="mixer",
         out_shape=(
-            jax.ShapeDtypeStruct((seqs, width), BF16),
+            pltpu.VMEM((seqs, width), BF16),
             jax.ShapeDtypeStruct(recur_state.shape, F32),
         ),
-        in_specs=[vmem] * 6 + [any_] * 6,
+        in_specs=[any_] * 12,
         out_specs=(vmem, any_),
-        scratch_shapes=[pltpu.VMEM((width, inner), BF16)] * 4
+        scratch_shapes=[pltpu.VMEM(small.shape, small.dtype) for small in smalls]
+        + [pltpu.VMEM((width, inner), BF16)] * 4
         + [
             pltpu.VMEM((inner, width), BF16),
             pltpu.VMEM((heads, seqs, hd, hd), F32),
             pltpu.VMEM((heads, seqs, hd, hd), F32),
-            dma((5,)),
+            dma((5 + len(smalls),)),
             dma((heads,)),
             dma((heads,)),
         ],
         compiler_params=pltpu.CompilerParams(vmem_limit_bytes=60 * 1024 * 1024),
     )(
-        tokens, attn_gain[None], beta_weight.T, decay_weight.T, decay_rate[None], head_gain[None],
-        key_weight, query_weight, value_weight, recur_state, outgate_weight, output_weight,
+        *smalls, key_weight, query_weight, value_weight, recur_state, outgate_weight, output_weight,
     )
     mixed = pl.pallas_call(
         functools.partial(expert_kernel, nz, ny, lanes),
         name="experts",
-        out_shape=jax.ShapeDtypeStruct((seqs, dl), BF16),
+        out_shape=pltpu.VMEM((seqs, dl), BF16),
         in_specs=[vmem] * 5 + [any_] * 3,
         out_specs=vmem,
         scratch_shapes=[
@@ -451,7 +462,7 @@
             collective_id=0, has_side_effects=True, vmem_limit_bytes=60 * 1024 * 1024
         ),
     )(
-        tokens, part, ffn_gain[None], routes.T, route_weight.T, expert_gate, expert_up, expert_down,
+        tokens, pltpu.with_memory_space_constraint(part, pltpu.VMEM), ffn_gain[None], routes.T, route_weight.T, expert_gate, expert_up, expert_down,
     )
     return mixed, new_state
 

time: 46.3 us -> 43.4 us (0.937)
  Pallas kernels: 44 us -> 42 us
  local copies, waits for them, and re-layouts: 1.38 us -> 0.62 us
    pallas_call x1, Pallas kernels: 8.05 us -> 6.72 us  [local(): pl.pallas_call(mixer_kernel, name='mixer', out_shape=(pltpu.VMEM((seqs, w...]
    unnamed x1, local copies, waits for them, and re-layouts: 1.38 us -> 0.62 us
    pallas_call x1, Pallas kernels: 35.9 us -> 35.3 us  [local(): pl.pallas_call(functools.partial(expert_kernel, nz, ny, lanes), name='exp...]
where the time goes in v3:
time: 43.4 us; the launch traced here: 43.3 us
  Pallas kernels  42 us (97%)
  between operations  0.65 us (1%)
  local copies, waits for them, and re-layouts  0.62 us (1%)
    pallas_call x1, Pallas kernels, local(): pl.pallas_call(functools.partial(expert_kernel, nz, ny, lanes), name='exp...  35.3 us
    pallas_call x1, Pallas kernels, local(): pl.pallas_call(mixer_kernel, name='mixer', out_shape=(pltpu.VMEM((seqs, w...  6.72 us

profile of v3, /device:TPU:0, one launch (start us, length us, event | category | flops | bytes accessed | tf_op | source)
XLA Modules:
  0.0 43.3 jit_solution(2883652695812089301)
XLA Ops:
  0.6 6.7 %mixer.1 = (bf16[16,2048]{1,0:T(8,128)(2,1)S(1)}, f32[16,4,128,128]{3,2,1,0:T(8,128)}) custom-call(bf16[16,2048]{1,0:T(8,128)(2,1)} %tok_ref.1, f32[1,2048]{1,0:T(1,128)} %bitcast.10, bf16[8,2048]{1,0:T(8,128)(2,1)} %bitcast.8, bf16[8,2048]{1,0:T(8,128)(2,1)} %bitcast.9, f32[1,8]{1,0:T(1,128)} %bitcast.14, f32[1,128]{1,0:T(1,128)} %bitcast.15, ...), custom_call_target="tpu_custom_call" | custom-call | tf_op jit(solution)/shard_map/mixer/pallas_call | solution.py:399
  7.4 35.3 %experts.1 = bf16[16,1024]{1,0:T(8,128)(2,1)S(1)} custom-call(bf16[16,2048]{1,0:T(8,128)(2,1)} %tok_ref.1, bf16[16,2048]{1,0:T(8,128)(2,1)S(1)} %get-tuple-element.4.part_ref, f32[1,2048]{1,0:T(1,128)} %bitcast.11, s32[2,16]{1,0:T(2,128)} %bitcast.12, f32[2,16]{1,0:T(2,128)} %bitcast.13, bf16[1,2048,512]{2,1,0:T(8,128)(2,1)} %wg_hbm.1, ...), custom_call_target="tpu_custom_call" | custom-call | tf_op jit(solution)/shard_map/experts/pallas_call | solution.py:422
  42.6 0.6 %copy.21 = bf16[16,1024]{1,0:T(8,128)(2,1)} copy(bf16[16,1024]{1,0:T(8,128)(2,1)S(1)} %experts.1) | data formatting | bytes 65536

commit v4 on v3

--- a/solution.py
+++ b/solution.py
@@ -122,8 +122,9 @@
 
 def expert_kernel(
     nz, ny, lanes,
-    tok_ref, part_ref, gain_ref, routes_ref, rw_ref, wg_hbm, wu_hbm, wd_hbm,
+    part_ref, tok_hbm, gain_hbm, routes_hbm, rw_hbm, wg_hbm, wu_hbm, wd_hbm,
     out_ref,
+    tok_ref, gain_ref, routes_ref, rw_ref,
     wg, wu, wd, tpb, rows, resid, cs, cr, pf, xs, xr, qf, ys, yr, ybs, ybr, zs, zr,
     w_sem, tp_s, tp_r, ag_s, ag_r, c_s, c_r, x_s, x_r, y_s, y_r, z_s, z_r,
 ):
@@ -136,6 +137,14 @@
     z = ep // (2 * ny)
     other = 1 - c
 
+    small = (
+        (tok_hbm, tok_ref), (gain_hbm, gain_ref), (routes_hbm, routes_ref), (rw_hbm, rw_ref),
+    )
+    first_in = []
+    for i, (src, dst) in enumerate(small):
+        copy = pltpu.make_async_copy(src, dst, w_sem.at[3 + i])
+        copy.start()
+        first_in.append(copy)
     fetched = []
     for i, (src, dst) in enumerate(((wg_hbm, wg), (wu_hbm, wu), (wd_hbm, wd))):
         copy = pltpu.make_async_copy(src.at[0], dst, w_sem.at[i])
@@ -176,6 +185,8 @@
     for d in range(1, lanes):
         send(part_ref, tpb.at[tp], tp_s.at[d], tp_r.at[tp], {"tp": turn(tp, d, lanes)})
 
+    for copy in first_in:
+        copy.wait()
     routes, weights = routes_ref[...].astype(F32), rw_ref[...]
     top = routes.shape[0]
     pad = jnp.zeros((8 - 2 * top % 8, seqs), F32)
@@ -419,13 +430,15 @@
     )(
         *smalls, key_weight, query_weight, value_weight, recur_state, outgate_weight, output_weight,
     )
+    smalls = (tokens, ffn_gain[None], routes.T, route_weight.T)
     mixed = pl.pallas_call(
         functools.partial(expert_kernel, nz, ny, lanes),
         name="experts",
         out_shape=pltpu.VMEM((seqs, dl), BF16),
-        in_specs=[vmem] * 5 + [any_] * 3,
+        in_specs=[vmem] + [any_] * 7,
         out_specs=vmem,
-        scratch_shapes=[
+        scratch_shapes=[pltpu.VMEM(small.shape, small.dtype) for small in smalls]
+        + [
             pltpu.VMEM((width, hidden), BF16),
             pltpu.VMEM((width, hidden), BF16),
             pltpu.VMEM((hidden, width), BF16),
@@ -444,7 +457,7 @@
             pltpu.VMEM((lanes, zy, seqs, dl), BF16),
             pltpu.VMEM((nz, seqs, dl), BF16),
             pltpu.VMEM((nz, seqs, dl), BF16),
-            dma((3,)),
+            dma((3 + len(smalls),)),
             dma((lanes,)),
             dma((lanes,)),
             dma((2 * (nz // 2) ** 2 + 2 * nz * (ny - 1) + 2 * zy,)),
@@ -462,7 +475,7 @@
             collective_id=0, has_side_effects=True, vmem_limit_bytes=60 * 1024 * 1024
         ),
     )(
-        tokens, pltpu.with_memory_space_constraint(part, pltpu.VMEM), ffn_gain[None], routes.T, route_weight.T, expert_gate, expert_up, expert_down,
+        pltpu.with_memory_space_constraint(part, pltpu.VMEM), *smalls, expert_gate, expert_up, expert_down,
     )
     return mixed, new_state
 

time: 43.4 us -> 42.6 us (0.982)
  Pallas kernels: 42 us -> 41.2 us
    pallas_call x1, Pallas kernels: 35.3 us -> 34.5 us  [local(): pl.pallas_call(functools.partial(expert_kernel, nz, ny, lanes), name='exp...]
where the time goes in v4:
time: 42.6 us; the launch traced here: 42.5 us
  Pallas kernels  41.2 us (97%)
  between operations  0.65 us (2%)
  local copies, waits for them, and re-layouts  0.62 us (1%)
    pallas_call x1, Pallas kernels, local(): pl.pallas_call(functools.partial(expert_kernel, nz, ny, lanes), name='exp...  34.5 us
    pallas_call x1, Pallas kernels, local(): pl.pallas_call(mixer_kernel, name='mixer', out_shape=(pltpu.VMEM((seqs, w...  6.72 us

profile of v4, /device:TPU:0, one launch (start us, length us, event | category | flops | bytes accessed | tf_op | source)
XLA Modules:
  0.0 42.5 jit_solution(13204872894957139830)
XLA Ops:
  0.6 6.7 %mixer.1 = (bf16[16,2048]{1,0:T(8,128)(2,1)S(1)}, f32[16,4,128,128]{3,2,1,0:T(8,128)}) custom-call(bf16[16,2048]{1,0:T(8,128)(2,1)} %tok_hbm.3, f32[1,2048]{1,0:T(1,128)} %bitcast.10, bf16[8,2048]{1,0:T(8,128)(2,1)} %bitcast.8, bf16[8,2048]{1,0:T(8,128)(2,1)} %bitcast.9, f32[1,8]{1,0:T(1,128)} %bitcast.14, f32[1,128]{1,0:T(1,128)} %bitcast.15, ...), custom_call_target="tpu_custom_call" | custom-call | tf_op jit(solution)/shard_map/mixer/pallas_call | solution.py:410
  7.4 34.5 %experts.1 = bf16[16,1024]{1,0:T(8,128)(2,1)S(1)} custom-call(bf16[16,2048]{1,0:T(8,128)(2,1)S(1)} %get-tuple-element.4.part_ref, bf16[16,2048]{1,0:T(8,128)(2,1)} %tok_hbm.3, f32[1,2048]{1,0:T(1,128)} %bitcast.11, s32[2,16]{1,0:T(2,128)} %bitcast.12, f32[2,16]{1,0:T(2,128)} %bitcast.13, bf16[1,2048,512]{2,1,0:T(8,128)(2,1)} %wg_hbm.1, ...), custom_call_target="tpu_custom_call" | custom-call | tf_op jit(solution)/shard_map/experts/pallas_call | solution.py:434
  41.9 0.6 %copy.21 = bf16[16,1024]{1,0:T(8,128)(2,1)} copy(bf16[16,1024]{1,0:T(8,128)(2,1)S(1)} %experts.1) | data formatting | bytes 65536
